TPU v7x, 32 devices: a whole 2x2x4 slice. The times are simulated.
32 devices in a mesh: grp: 2 (over y), sp: 4 (over z), tp: 4 (over x, core).
Axes of the slice: x: 2, y: 2, z: 4, core: 2. Of those that a mesh axis runs over, the one named last changes fastest.
Arguments:
- queries: bfloat16 [1024, 2048], P(('grp', 'sp'), 'tp'), parts along dimension 0, may hold values from -8 to 8
- keys: bfloat16 [1024, 1024], P(('grp', 'sp'), 'tp'), parts along dimension 0, may hold values from -6 to 6
- values: bfloat16 [1024, 1024], P(('grp', 'sp'), 'tp'), parts along dimension 0, may hold values from -6 to 6
- head_bias: float32 [16], P('tp'), may hold values from -15 to -5
- documents: int32 [1024], P(('grp', 'sp')), parts along dimension 0, may hold values from 0 to 2, never falling along the last dimension, each value on 1 to 384 neighbouring positions
- w_out: bfloat16 [2048, 2048], P('tp'), may hold values from -0.125 to 0.125
- resid: bfloat16 [1024, 2048], P(('grp', 'sp', 'tp')), parts along dimension 0, may hold values from -6 to 6
- norm_gain: float32 [2048], replicated, may hold values from 0.1 to 1.9
- expert_ids: int32 [1024, 2], P(('grp', 'sp', 'tp')), parts along dimension 0, may hold values from 0 to 3, all different within a row; in each aligned block of 32 rows (0 to 31, 32 to 63, ...) at most 32 rows name the same one
- expert_gates: float32 [1024, 2], P(('grp', 'sp', 'tp')), parts along dimension 0, may hold values from 0.1 to 0.9
- w_gate: bfloat16 [4, 2048, 3072], P('sp', None, 'tp'), may hold values from -0.125 to 0.125
- w_up: bfloat16 [4, 2048, 3072], P('sp', None, 'tp'), may hold values from -0.125 to 0.125
- w_down: bfloat16 [4, 3072, 2048], P('sp', 'tp'), may hold values from -0.109375 to 0.109375
Outputs:
- layer_out: bfloat16 [1024, 2048], P(('grp', 'sp', 'tp')), parts along dimension 0
There are 2 independent parts, one for each index of `grp`. A program takes and returns all parts, laid end to end along the dimension named above; an argument that names none is the same for every part. Nothing has to cross between parts.
Inputs may be any that keep to these rules, and one draw needn't show every extreme that they name: Document numbers never fall along the sequence; each of the 3 documents holds at least one position and the longest exactly 384 positions. `expert_ids`: each position names 2 different experts. Among the 32 positions of one device (aligned blocks of 32 rows) no expert is named more than 32 times, and in some block some expert exactly 32 times.
All inputs are finite; a program needn't handle non-finite values.
Results may differ from a plain program's by a relative error of at most 0.012.
Values may be sent and summed in bfloat16 or wider, within the bound.
No kernel may reach another device: no remote copies, remote signals or barrier semaphores. Data moves between devices by JAX's collectives and lax.ppermute only.
A program may use at most 64 MiB of HBM per device.

v0:
```python
import jax
import jax.numpy as jnp
from jax import lax
from jax.sharding import PartitionSpec as P

D = 2048
HEADS = 16
KV_HEADS = 8
DH = 128
TOPK = 2


def passed_along(value, axis, steps):
    count = lax.axis_size(axis)
    initial, last = (max(0, -steps), min(count, count - steps))
    return lax.ppermute(value, axis, [(source, source + steps) for source in range(initial, last)])


def attend_terms(query_grid, bias_grid, key_block, value_block, live, carried):
    kv_local = bias_grid.shape[0]
    key_count = key_block.shape[0]
    logits = (
        jnp.einsum(
            "qgrd,sgd->grqs",
            query_grid,
            key_block.reshape(key_count, kv_local, DH),
            preferred_element_type=jnp.float32,
        )
        * DH ** (-0.5)
        + bias_grid[:, :, None, None]
    )
    keep = jnp.where(live, jax.nn.log_sigmoid(-logits), 0.0)
    after = lax.cumsum(keep, axis=3, reverse=True) - keep + carried[:, :, :, None]
    weight = jnp.where(live, jnp.exp(jax.nn.log_sigmoid(logits) + after), 0.0).astype(jnp.bfloat16)
    partial_mix = jnp.einsum(
        "grqs,sgd->qgrd",
        weight,
        value_block.reshape(key_count, kv_local, DH),
        preferred_element_type=jnp.float32,
    )
    return (partial_mix, jnp.sum(keep, axis=3))


def local(
    queries,
    keys,
    values,
    head_bias,
    documents,
    w_out,
    resid,
    norm_gain,
    expert_ids,
    expert_gates,
    w_gate,
    w_up,
    w_down,
):
    tok_count = queries.shape[0]
    kv_local = keys.shape[1] // DH
    group_size = HEADS // KV_HEADS
    sp_count = lax.axis_size("sp")
    tp_count = lax.axis_size("tp")
    sp_index = lax.axis_index("sp")
    query_grid = queries.reshape(tok_count, kv_local, group_size, DH)
    bias_grid = head_bias.reshape(kv_local, group_size)
    doc_here = documents.astype(jnp.bfloat16)
    doc_column = doc_here.reshape(tok_count, 1)
    local_pos = jnp.arange(tok_count, dtype=jnp.int32)
    live_local = (local_pos[None, :] < local_pos[:, None]) & (
        documents[None, :] == documents[:, None]
    )
    zero_carry = jnp.zeros((kv_local, group_size, tok_count), jnp.float32)
    mix_total, carried = attend_terms(query_grid, bias_grid, keys, values, live_local, zero_carry)

    def visit(turn_index, state):
        mix_sum, carry_sum, key_block, value_block, doc_block = state
        key_block, value_block, doc_block = passed_along(
            (key_block, value_block, doc_block), "sp", 1
        )
        live = (doc_block[:, 0][None, :] == doc_here[:, None]) & (sp_index - turn_index >= 0)
        partial_mix, block_keep = attend_terms(
            query_grid, bias_grid, key_block, value_block, live, carry_sum
        )
        return (mix_sum + partial_mix, carry_sum + block_keep, key_block, value_block, doc_block)

    mix_total, carried, key_last, value_last, doc_last = lax.fori_loop(
        1, sp_count, visit, (mix_total, carried, keys, values, doc_column)
    )
    mixed = mix_total.reshape(tok_count, kv_local * group_size * DH).astype(jnp.bfloat16)
    projected = lax.psum_scatter(
        jnp.dot(mixed, w_out, preferred_element_type=jnp.float32).astype(jnp.bfloat16),
        "tp",
        scatter_dimension=0,
        tiled=True,
    ).astype(jnp.float32)
    middle = (resid.astype(jnp.float32) + projected).astype(jnp.bfloat16)
    middle_value = middle.astype(jnp.float32)
    normed = (
        middle_value
        * lax.rsqrt(jnp.mean(middle_value * middle_value, axis=1, keepdims=True) + 1e-06)
        * norm_gain
    ).astype(jnp.bfloat16)
    row_count = normed.shape[0]
    expert_count = w_gate.shape[0] * sp_count
    slot_limit = min(row_count, max(2, 2 * TOPK * row_count // expert_count))
    flat_ids = expert_ids.reshape(-1)
    onehot_ids = (flat_ids[:, None] == jnp.arange(expert_count, dtype=jnp.int32)[None, :]).astype(
        jnp.int32
    )
    earlier = jnp.cumsum(onehot_ids, axis=0) - onehot_ids
    slot_ids = jnp.sum(earlier * onehot_ids, axis=1)
    target = flat_ids * slot_limit + slot_ids
    placing = (
        jnp.arange(expert_count * slot_limit, dtype=jnp.int32)[:, None] == target[None, :]
    ).astype(jnp.bfloat16)
    by_token = jnp.sum(placing.reshape(expert_count * slot_limit, row_count, TOPK), axis=2)
    outgoing = jnp.dot(by_token, normed, preferred_element_type=jnp.float32).astype(jnp.bfloat16)
    outgoing = outgoing.reshape(expert_count, slot_limit, D)
    arrived = lax.all_to_all(outgoing, "sp", split_axis=0, concat_axis=0, tiled=True)
    gathered = lax.all_gather(arrived, "tp", axis=0, tiled=True)
    expert_rows = gathered.reshape(-1, D)
    gate_value = jnp.dot(expert_rows, w_gate[0], preferred_element_type=jnp.float32)
    up_value = jnp.dot(expert_rows, w_up[0], preferred_element_type=jnp.float32)
    hidden = (jax.nn.silu(gate_value) * up_value).astype(jnp.bfloat16)
    partial_out = jnp.dot(hidden, w_down[0], preferred_element_type=jnp.float32)
    summed = lax.psum_scatter(
        partial_out.reshape(tp_count, sp_count * slot_limit, D).astype(jnp.bfloat16),
        "tp",
        scatter_dimension=0,
        tiled=True,
    ).astype(jnp.float32)
    expert_result = summed.reshape(sp_count, slot_limit, D).astype(jnp.bfloat16)
    returned = lax.all_to_all(expert_result, "sp", split_axis=0, concat_axis=0, tiled=True)
    routed = jnp.dot(placing.T, returned.reshape(-1, D), preferred_element_type=jnp.float32)
    combined = jnp.sum(expert_gates[:, :, None] * routed.reshape(row_count, TOPK, D), axis=1)
    return (middle_value + combined).astype(jnp.bfloat16)


def solution(mesh):
    return jax.shard_map(
        local,
        mesh=mesh,
        in_specs=(
            P(("grp", "sp"), "tp"),
            P(("grp", "sp"), "tp"),
            P(("grp", "sp"), "tp"),
            P("tp"),
            P(("grp", "sp")),
            P("tp", None),
            P(("grp", "sp", "tp"), None),
            P(),
            P(("grp", "sp", "tp"), None),
            P(("grp", "sp", "tp"), None),
            P("sp", None, "tp"),
            P("sp", None, "tp"),
            P("sp", "tp", None),
        ),
        out_specs=P(("grp", "sp", "tp"), None),
        check_vma=False,
    )
```

profile of v0, /device:TPU:0, one launch (start us, length us, event | category | flops | bytes accessed | tf_op | source)
XLA Modules:
  0.0 232.2 jit_solution(13194715823110891600)
XLA Ops:
  6.5 0.9 fusion.50
  7.5 1.3 fusion.58
  8.8 1.5 reshape.106
  10.2 1.6 copy.78
  11.8 1.5 reshape.108
  13.3 1.6 copy.79
  14.8 1.0 copy.73
  15.9 1.3 add.157
  17.1 0.8 copy.80
  17.9 2.4 %fusion.56 = (f32[2,2,128]{2,1,0:T(2,128)}, f32[2,2,128,128]{2,3,1,0:T(8,128)S(1)}, f32[2,2,128,128]{2,3,1,0:T(8,128)}) fusion(pred[128,128]{0,1:T(8,128)(4,1)S(1)} %fusion.50, f32[2,2]{1,0:T(2,128)} %add.157, bf16[128,2,2,128]{0,3,2,1:T(8,128)(2,1)S(1)} %bitcast.78, bf16[128,2,128,1]{2,1,0,3:T(2,128)(2,1)} %bitcast.81), kind=kOutput, calls=%fused_computation.74 | convolution fusion | flops 17497600 | bytes 739344 | tf_op jit(solution)/shard_map/qgrd,sgd->grqs/dot_general | solution.py:23
  20.3 5.1 %reduce_window_sum.31 = f32[2,2,128,128]{2,3,1,0:T(8,128)} reduce-window(f32[2,2,128,128]{2,3,1,0:T(8,128)S(1)} %get-tuple-element.239, f32[]{:T(128)} %constant.57.clone.1), window={size=1x1x1x128 pad=0_0x0_0x0_0x0_127}, to_apply=%region_0.1 | reduce-window | flops 8323072 | bytes 524292 | tf_op jit(solution)/shard_map/attend_terms/reduce_window_sum | solution.py:33
  25.5 2.3 convolution_bitcast_fusion.1
  27.7 69.8 %while.21 = (s32[]{:T(128)}, f32[128,2,2,128]{3,0,2,1:T(8,128)}, f32[2,2,128]{2,1,0:T(2,128)}, bf16[128,256]{0,1:T(8,128)(2,1)}, bf16[128,256]{0,1:T(8,128)(2,1)...) while((s32[]{:T(128)}, f32[128,2,2,128]{3,0,2,1:T(8,128)}, ...), condition=%wide.region_5.6_spmd, body=%wide.region_2.5_spmd.sunk | while | flops 44105732 | bytes 3207487 | solution.py:87
  27.7 4.9 %collective-permute-start.1 = (bf16[128,1]{0,1:T(2,128)(2,1)}, bf16[128,1]{0,1:T(2,128)(2,1)S(1)}, u32[]{:S(2)}, u32[]{:S(2)}) collective-permute-start(bf16[128,1]{0,1:T(2,128)(2,1)} %get-tuple-element.328), channel_id=1, source_target_pairs={{0,4},{4,8},{8,12},{1,5},{5,9},{9,13},{2,6},{6,10},{10,14},{3,7},{... | collective-permute-start | bytes 776 | tf_op jit(solution)/shard_map/while/body/eval_jaxpr/ppermute | solution.py:16
  32.7 3.5 %collective-permute-start.2 = (bf16[128,256]{0,1:T(8,128)(2,1)}, bf16[128,256]{0,1:T(8,128)(2,1)S(1)}, u32[]{:S(2)}, u32[]{:S(2)}) collective-permute-start(bf16[128,256]{0,1:T(8,128)(2,1)} %get-tuple-element.326), channel_id=1, source_target_pairs={{0,4},{4,8},{8,12},{1,5},{5,9},{9,13},{2,6},{6,10},{10,14},{3,7},{... | collective-permute-start | bytes 196616 | tf_op jit(solution)/shard_map/while/body/eval_jaxpr/ppermute | solution.py:16
  36.2 3.5 %collective-permute-start = (bf16[128,256]{0,1:T(8,128)(2,1)}, bf16[128,256]{0,1:T(8,128)(2,1)S(1)}, u32[]{:S(2)}, u32[]{:S(2)}) collective-permute-start(bf16[128,256]{0,1:T(8,128)(2,1)} %get-tuple-element.327), channel_id=1, source_target_pairs={{0,4},{4,8},{8,12},{1,5},{5,9},{9,13},{2,6},{6,10},{10,14},{3,7},{... | collective-permute-start | bytes 196616 | tf_op jit(solution)/shard_map/while/body/eval_jaxpr/ppermute | solution.py:16
  41.7 2.6 %fusion.80 = (f32[2,2,128]{2,1,0:T(2,128)}, f32[2,2,128,128]{2,3,1,0:T(8,128)}, f32[2,2,128,128]{2,3,1,0:T(8,128)}) fusion(pred[128,128]{0,1:T(8,128)(4,1)S(1)} %compare_and_fusion.2, f32[2,2]{1,0:T(2,128)S(1)} %add.252, bf16[128,2,128,1]{0,2,3,1:T(8,128)(2,1)S(1)} %bitcast.74, bf16[128,2,2,128]{3,0,2,1:T(8,128)(2,1)} %get-tuple-element.344), kind=kOutput, calls=%fused_computation.19.clone.1 | convolution fusion | flops 17497600 | bytes 739344 | tf_op jit(solution)/shard_map/while/body/eval_jaxpr/qgrd,sgd->grqs/dot_general | solution.py:23
  44.3 5.4 %reduce_window_sum.34 = f32[2,2,128,128]{2,3,1,0:T(8,128)S(1)} reduce-window(f32[2,2,128,128]{2,3,1,0:T(8,128)} %get-tuple-element.307, f32[]{:T(128)} %constant.57.clone.1..sunk), window={size=1x1x1x128 pad=0_0x0_0x0_0x0_127}, to_apply=%region_3.3 | reduce-window | flops 8323072 | bytes 524292 | tf_op jit(solution)/shard_map/while/body/eval_jaxpr/reduce_window_sum | solution.py:33
  49.7 2.3 fusion.81
  52.0 1.3 add.253
  54.5 1.9 collective-permute-start.1
  56.4 2.6 %collective-permute-start.2 = (bf16[128,256]{0,1:T(8,128)(2,1)}, bf16[128,256]{0,1:T(8,128)(2,1)S(1)}, u32[]{:S(2)}, u32[]{:S(2)}) collective-permute-start(bf16[128,256]{0,1:T(8,128)(2,1)} %get-tuple-element.326), channel_id=1, source_target_pairs={{0,4},{4,8},{8,12},{1,5},{5,9},{9,13},{2,6},{6,10},{10,14},{3,7},{... | collective-permute-start | bytes 196616 | tf_op jit(solution)/shard_map/while/body/eval_jaxpr/ppermute | solution.py:16
  59.0 1.9 collective-permute-start
  63.0 2.6 %fusion.80 = (f32[2,2,128]{2,1,0:T(2,128)}, f32[2,2,128,128]{2,3,1,0:T(8,128)}, f32[2,2,128,128]{2,3,1,0:T(8,128)}) fusion(pred[128,128]{0,1:T(8,128)(4,1)S(1)} %compare_and_fusion.2, f32[2,2]{1,0:T(2,128)S(1)} %add.252, bf16[128,2,128,1]{0,2,3,1:T(8,128)(2,1)S(1)} %bitcast.74, bf16[128,2,2,128]{3,0,2,1:T(8,128)(2,1)} %get-tuple-element.344), kind=kOutput, calls=%fused_computation.19.clone.1 | convolution fusion | flops 17497600 | bytes 739344 | tf_op jit(solution)/shard_map/while/body/eval_jaxpr/qgrd,sgd->grqs/dot_general | solution.py:23
  65.6 5.4 %reduce_window_sum.34 = f32[2,2,128,128]{2,3,1,0:T(8,128)S(1)} reduce-window(f32[2,2,128,128]{2,3,1,0:T(8,128)} %get-tuple-element.307, f32[]{:T(128)} %constant.57.clone.1..sunk), window={size=1x1x1x128 pad=0_0x0_0x0_0x0_127}, to_apply=%region_3.3 | reduce-window | flops 8323072 | bytes 524292 | tf_op jit(solution)/shard_map/while/body/eval_jaxpr/reduce_window_sum | solution.py:33
  71.0 2.3 fusion.81
  73.3 1.3 add.253
  75.8 2.7 %collective-permute-start.1 = (bf16[128,1]{0,1:T(2,128)(2,1)}, bf16[128,1]{0,1:T(2,128)(2,1)S(1)}, u32[]{:S(2)}, u32[]{:S(2)}) collective-permute-start(bf16[128,1]{0,1:T(2,128)(2,1)} %get-tuple-element.328), channel_id=1, source_target_pairs={{0,4},{4,8},{8,12},{1,5},{5,9},{9,13},{2,6},{6,10},{10,14},{3,7},{... | collective-permute-start | bytes 776 | tf_op jit(solution)/shard_map/while/body/eval_jaxpr/ppermute | solution.py:16
  78.5 2.2 collective-permute-start.2
  80.7 2.0 collective-permute-start
  84.7 2.6 %fusion.80 = (f32[2,2,128]{2,1,0:T(2,128)}, f32[2,2,128,128]{2,3,1,0:T(8,128)}, f32[2,2,128,128]{2,3,1,0:T(8,128)}) fusion(pred[128,128]{0,1:T(8,128)(4,1)S(1)} %compare_and_fusion.2, f32[2,2]{1,0:T(2,128)S(1)} %add.252, bf16[128,2,128,1]{0,2,3,1:T(8,128)(2,1)S(1)} %bitcast.74, bf16[128,2,2,128]{3,0,2,1:T(8,128)(2,1)} %get-tuple-element.344), kind=kOutput, calls=%fused_computation.19.clone.1 | convolution fusion | flops 17497600 | bytes 739344 | tf_op jit(solution)/shard_map/while/body/eval_jaxpr/qgrd,sgd->grqs/dot_general | solution.py:23
  87.3 5.4 %reduce_window_sum.34 = f32[2,2,128,128]{2,3,1,0:T(8,128)S(1)} reduce-window(f32[2,2,128,128]{2,3,1,0:T(8,128)} %get-tuple-element.307, f32[]{:T(128)} %constant.57.clone.1..sunk), window={size=1x1x1x128 pad=0_0x0_0x0_0x0_127}, to_apply=%region_3.3 | reduce-window | flops 8323072 | bytes 524292 | tf_op jit(solution)/shard_map/while/body/eval_jaxpr/reduce_window_sum | solution.py:33
  92.7 2.3 fusion.81
  95.0 1.3 add.253
  97.5 1.1 copy.81
  98.6 2.9 %convolution_convert_fusion.1 = bf16[128,2048]{1,0:T(8,128)(2,1)} fusion(bf16[128,512]{0,1:T(8,128)(2,1)S(1)} %bitcast.79, bf16[512,2048]{1,0:T(8,128)(2,1)} %param.20), kind=kOutput, calls=%fused_computation.28 | convolution fusion | flops 268697600 | bytes 2752512 | tf_op jit(solution)/shard_map/dot_general | solution.py:92
  102.6 19.0 %reduce-scatter.3.cloned.1.call-done = bf16[32,2048]{1,0:T(8,128)(2,1)} async-done(((bf16[128,2048]{1,0:T(8,128)(2,1)}), bf16[32,2048]{1,0:T(8,128)(2,1)}) %reduce-scatter.3.cloned.1.call-update) | async-done | bytes 131088 | tf_op jit(solution)/shard_map/reduce_scatter | solution.py:91
  121.6 1.1 fusion.31
  122.7 1.2 convolution_convert_fusion
  123.9 18.8 %all_to_all.10 = bf16[4,32,2048]{2,1,0:T(8,128)(2,1)} all-to-all(bf16[4,32,2048]{2,1,0:T(8,128)(2,1)S(1)} %bitcast.73), channel_id=1, replica_groups=mesh['grp'=2,'sp'=4,'tp'=4] {'sp'}, dimensions={0} | all-to-all | bytes 1048576 | tf_op jit(solution)/shard_map/all_to_all | solution.py:120
  142.8 20.8 %all-gather.2.cloned.1.call-done = bf16[16,32,2048]{2,1,0:T(8,128)(2,1)} async-done(((bf16[4,32,2048]{2,1,0:T(8,128)(2,1)}), bf16[16,32,2048]{2,1,0:T(8,128)(2,1)}) %all-gather.2.cloned.1.call-update) | async-done | bytes 2097168 | tf_op jit(solution)/shard_map/all_gather | solution.py:121
  163.6 4.5 %fusion.21 = f32[512,768]{1,0:T(8,128)S(1)} fusion(bf16[512,2048]{1,0:T(8,128)(2,1)} %bitcast.83, bf16[1,2048,768]{2,1,0:T(8,128)(2,1)} %param.25), kind=kOutput, calls=%fused_computation.24 | convolution fusion | flops 1610612736 | bytes 6815744 | tf_op jit(solution)/shard_map/dot_general | solution.py:123
  168.1 1.9 multiply_convert_fusion
  170.0 3.2 %fusion.23 = bf16[4,128,2048]{2,1,0:T(8,128)(2,1)} fusion(bf16[4,128,768]{2,1,0:T(8,128)(2,1)S(1)} %bitcast.85, bf16[1,768,2048]{2,1,0:T(8,128)(2,1)S(1)} %copy-done), kind=kOutput, calls=%fused_computation.26 | convolution fusion | flops 1611661312 | bytes 6029312 | tf_op jit(solution)/shard_map/dot_general | solution.py:126
  173.3 31.3 %reduce-scatter.5.cloned.1.call-done = bf16[1,128,2048]{2,1,0:T(8,128)(2,1)} async-done(((bf16[4,128,2048]{2,1,0:T(8,128)(2,1)}), bf16[1,128,2048]{2,1,0:T(8,128)(2,1)}) %reduce-scatter.5.cloned.1.call-update) | async-done | bytes 524304 | tf_op jit(solution)/shard_map/reduce_scatter | solution.py:127
  204.6 4.6 %all-to-all-start.1 = ((bf16[4,32,2048]{2,1,0:T(8,128)(2,1)}), bf16[4,32,2048]{2,1,0:T(8,128)(2,1)}, u32[]{:S(2)}, u32[]{:S(2)}) async-start(bf16[4,32,2048]{2,1,0:T(8,128)(2,1)} %bitcast.76), calls=%async_computation.3 | async-start | bytes 1048576 | tf_op jit(solution)/shard_map/all_to_all | solution.py:134
  209.3 14.3 %all-to-all-done.1 = bf16[4,32,2048]{2,1,0:T(8,128)(2,1)} async-done(((bf16[4,32,2048]{2,1,0:T(8,128)(2,1)}), bf16[4,32,2048]{2,1,0:T(8,128)(2,1)}, u32[]{:S(2)}, u32[]{:S(2)}) %all-to-all-start.1) | async-done | bytes 524320 | tf_op jit(solution)/shard_map/all_to_all | solution.py:134
  223.6 1.3 fusion.28
  (60 shorter events, 11.7 us)
Async XLA Ops:
  6.5 163.5 %copy-start = (bf16[1,768,2048]{2,1,0:T(8,128)(2,1)S(1)}, bf16[1,768,2048]{2,1,0:T(8,128)(2,1)}, u32[]{:S(2)}) copy-start(bf16[1,768,2048]{2,1,0:T(8,128)(2,1)} %param.27) | copy-start | bytes 9437188
  6.5 115.0 %reduce-scatter.3.cloned.1.call-start = ((), (), s32[]{:S(2)}) async-start(), calls=%async_computation.4 | async-start | bytes 655360 | tf_op jit(solution)/shard_map/reduce_scatter | solution.py:91
  27.7 12.7 %collective-permute-start.1 = (bf16[128,1]{0,1:T(2,128)(2,1)}, bf16[128,1]{0,1:T(2,128)(2,1)S(1)}, u32[]{:S(2)}, u32[]{:S(2)}) collective-permute-start(bf16[128,1]{0,1:T(2,128)(2,1)} %get-tuple-element.328), channel_id=1, source_target_pairs={{0,4},{4,8},{8,12},{1,5},{5,9},{9,13},{2,6},{6,10},{10,14},{3,7},{... | collective-permute-start | bytes 776 | tf_op jit(solution)/shard_map/while/body/eval_jaxpr/ppermute | solution.py:16
  32.7 9.0 %collective-permute-start.2 = (bf16[128,256]{0,1:T(8,128)(2,1)}, bf16[128,256]{0,1:T(8,128)(2,1)S(1)}, u32[]{:S(2)}, u32[]{:S(2)}) collective-permute-start(bf16[128,256]{0,1:T(8,128)(2,1)} %get-tuple-element.326), channel_id=1, source_target_pairs={{0,4},{4,8},{8,12},{1,5},{5,9},{9,13},{2,6},{6,10},{10,14},{3,7},{... | collective-permute-start | bytes 196616 | tf_op jit(solution)/shard_map/while/body/eval_jaxpr/ppermute | solution.py:16
  36.2 13.5 %collective-permute-start = (bf16[128,256]{0,1:T(8,128)(2,1)}, bf16[128,256]{0,1:T(8,128)(2,1)S(1)}, u32[]{:S(2)}, u32[]{:S(2)}) collective-permute-start(bf16[128,256]{0,1:T(8,128)(2,1)} %get-tuple-element.327), channel_id=1, source_target_pairs={{0,4},{4,8},{8,12},{1,5},{5,9},{9,13},{2,6},{6,10},{10,14},{3,7},{... | collective-permute-start | bytes 196616 | tf_op jit(solution)/shard_map/while/body/eval_jaxpr/ppermute | solution.py:16
  54.5 7.2 %collective-permute-start.1 = (bf16[128,1]{0,1:T(2,128)(2,1)}, bf16[128,1]{0,1:T(2,128)(2,1)S(1)}, u32[]{:S(2)}, u32[]{:S(2)}) collective-permute-start(bf16[128,1]{0,1:T(2,128)(2,1)} %get-tuple-element.328), channel_id=1, source_target_pairs={{0,4},{4,8},{8,12},{1,5},{5,9},{9,13},{2,6},{6,10},{10,14},{3,7},{... | collective-permute-start | bytes 776 | tf_op jit(solution)/shard_map/while/body/eval_jaxpr/ppermute | solution.py:16
  56.4 6.6 %collective-permute-start.2 = (bf16[128,256]{0,1:T(8,128)(2,1)}, bf16[128,256]{0,1:T(8,128)(2,1)S(1)}, u32[]{:S(2)}, u32[]{:S(2)}) collective-permute-start(bf16[128,256]{0,1:T(8,128)(2,1)} %get-tuple-element.326), channel_id=1, source_target_pairs={{0,4},{4,8},{8,12},{1,5},{5,9},{9,13},{2,6},{6,10},{10,14},{3,7},{... | collective-permute-start | bytes 196616 | tf_op jit(solution)/shard_map/while/body/eval_jaxpr/ppermute | solution.py:16
  59.0 12.0 %collective-permute-start = (bf16[128,256]{0,1:T(8,128)(2,1)}, bf16[128,256]{0,1:T(8,128)(2,1)S(1)}, u32[]{:S(2)}, u32[]{:S(2)}) collective-permute-start(bf16[128,256]{0,1:T(8,128)(2,1)} %get-tuple-element.327), channel_id=1, source_target_pairs={{0,4},{4,8},{8,12},{1,5},{5,9},{9,13},{2,6},{6,10},{10,14},{3,7},{... | collective-permute-start | bytes 196616 | tf_op jit(solution)/shard_map/while/body/eval_jaxpr/ppermute | solution.py:16
  75.8 7.6 %collective-permute-start.1 = (bf16[128,1]{0,1:T(2,128)(2,1)}, bf16[128,1]{0,1:T(2,128)(2,1)S(1)}, u32[]{:S(2)}, u32[]{:S(2)}) collective-permute-start(bf16[128,1]{0,1:T(2,128)(2,1)} %get-tuple-element.328), channel_id=1, source_target_pairs={{0,4},{4,8},{8,12},{1,5},{5,9},{9,13},{2,6},{6,10},{10,14},{3,7},{... | collective-permute-start | bytes 776 | tf_op jit(solution)/shard_map/while/body/eval_jaxpr/ppermute | solution.py:16
  78.5 6.2 %collective-permute-start.2 = (bf16[128,256]{0,1:T(8,128)(2,1)}, bf16[128,256]{0,1:T(8,128)(2,1)S(1)}, u32[]{:S(2)}, u32[]{:S(2)}) collective-permute-start(bf16[128,256]{0,1:T(8,128)(2,1)} %get-tuple-element.326), channel_id=1, source_target_pairs={{0,4},{4,8},{8,12},{1,5},{5,9},{9,13},{2,6},{6,10},{10,14},{3,7},{... | collective-permute-start | bytes 196616 | tf_op jit(solution)/shard_map/while/body/eval_jaxpr/ppermute | solution.py:16
  80.7 12.0 %collective-permute-start = (bf16[128,256]{0,1:T(8,128)(2,1)}, bf16[128,256]{0,1:T(8,128)(2,1)S(1)}, u32[]{:S(2)}, u32[]{:S(2)}) collective-permute-start(bf16[128,256]{0,1:T(8,128)(2,1)} %get-tuple-element.327), channel_id=1, source_target_pairs={{0,4},{4,8},{8,12},{1,5},{5,9},{9,13},{2,6},{6,10},{10,14},{3,7},{... | collective-permute-start | bytes 196616 | tf_op jit(solution)/shard_map/while/body/eval_jaxpr/ppermute | solution.py:16
  97.5 4.2 %copy-start.4 = (s32[32,2]{0,1:T(2,128)S(1)}, s32[32,2]{0,1:T(2,128)}, u32[]{:S(2)}) copy-start(s32[32,2]{0,1:T(2,128)} %param.23) | copy-start | bytes 772
  97.5 24.1 %copy-start.1 = (bf16[32,2048]{1,0:T(8,128)(2,1)S(1)}, bf16[32,2048]{1,0:T(8,128)(2,1)}, u32[]{:S(2)}) copy-start(bf16[32,2048]{1,0:T(8,128)(2,1)} %param.21) | copy-start | bytes 393220
  97.5 25.1 %copy-start.3 = (f32[2048]{0:T(1024)S(1)}, f32[2048]{0:T(1024)}, u32[]{:S(2)}) copy-start(f32[2048]{0:T(1024)} %param.22) | copy-start | bytes 24580
  101.5 62.1 %all-gather.2.cloned.1.call-start = ((), (), s32[]{:S(2)}) async-start(), calls=%async_computation.5 | async-start | bytes 2621440 | tf_op jit(solution)/shard_map/all_gather | solution.py:121
  142.8 61.8 %reduce-scatter.5.cloned.1.call-start = ((), (), s32[]{:S(2)}) async-start(), calls=%async_computation.6 | async-start | bytes 2621440 | tf_op jit(solution)/shard_map/reduce_scatter | solution.py:127
  163.6 4.5 %copy-start.6 = (bf16[1,2048,768]{2,1,0:T(8,128)(2,1)S(1)}, bf16[1,2048,768]{2,1,0:T(8,128)(2,1)}, u32[]{:S(2)}) copy-start(bf16[1,2048,768]{2,1,0:T(8,128)(2,1)} %param.26) | copy-start | bytes 9437188
  163.6 4.5 %copy-start.7 = (bf16[16,32,2048]{2,1,0:T(8,128)(2,1)S(1)}, bf16[16,32,2048]{2,1,0:T(8,128)(2,1)}, u32[]{:S(2)}) copy-start(bf16[16,32,2048]{2,1,0:T(8,128)(2,1)} %all-gather.2.cloned.1.call-done) | copy-start | bytes 6291460
  173.2 50.4 %copy-start.5 = (f32[32,2]{0,1:T(2,128)S(1)}, f32[32,2]{0,1:T(2,128)}, u32[]{:S(2)}) copy-start(f32[32,2]{0,1:T(2,128)} %param.24) | copy-start | bytes 772
  173.2 51.7 %copy-start.2 = (bf16[32,2048]{1,0:T(8,128)(2,1)S(1)}, bf16[32,2048]{1,0:T(8,128)(2,1)}, u32[]{:S(2)}) copy-start(bf16[32,2048]{1,0:T(8,128)(2,1)} %reduce-scatter.3.cloned.1.call-done) | copy-start | bytes 393220
  204.6 19.1 %all-to-all-start.1 = ((bf16[4,32,2048]{2,1,0:T(8,128)(2,1)}), bf16[4,32,2048]{2,1,0:T(8,128)(2,1)}, u32[]{:S(2)}, u32[]{:S(2)}) async-start(bf16[4,32,2048]{2,1,0:T(8,128)(2,1)} %bitcast.76), calls=%async_computation.3 | async-start | bytes 1048576 | tf_op jit(solution)/shard_map/all_to_all | solution.py:134
Sparse Core Ops, SparseCore 0:
  101.7 19.8 reduce-scatter.2
  142.9 20.6 all-gather.1
  173.4 31.1 reduce-scatter.4
where the time goes:
time: 233 us; the launch traced here: 232 us
  waiting for transfers between devices  85.5 us (37%)
  matrix products  34.5 us (15%)
  other arithmetic  31.5 us (14%)
  starting transfers between devices  30.1 us (13%)
  blocking collectives  18.8 us (8%)
  local copies, waits for them, and re-layouts  18.3 us (8%)
  between operations  13.2 us (6%)
    reduce_scatter x1, waiting for transfers between devices, local(): lax.psum_scatter(partial_out.reshape(tp_count, sp_count * slot_limit, D)....  31.3 us
    ppermute x9, starting transfers between devices, passed_along(): lax.ppermute(value, axis, [(source, source + steps) for source in range(i...  25.2 us
    another operation x4, other arithmetic, attend_terms(): lax.cumsum(keep, axis=3, reverse=True) - keep + carried[:, :, :, None]  21.2 us
    all_gather x1, waiting for transfers between devices, local(): gathered = lax.all_gather(arrived, 'tp', axis=0, tiled=True)  20.8 us
    reduce_scatter x1, waiting for transfers between devices, local(): lax.psum_scatter(jnp.dot(mixed, w_out, preferred_element_type=jnp.float32...  19 us
    all_to_all x1, blocking collectives, local(): lax.all_to_all(outgoing, 'sp', split_axis=0, concat_axis=0, tiled=True)  18.8 us
    all_to_all x1, waiting for transfers between devices, local(): lax.all_to_all(expert_result, 'sp', split_axis=0, concat_axis=0, tiled=True)  14.3 us
    dot_general x4, matrix products, attend_terms(): jnp.einsum('qgrd,sgd->grqs', query_grid, key_block.reshape(key_count, kv_...  10.4 us
  transfers between devices with their start and end apart: 13, of which 4 were waited for; matrix products, arithmetic and copies ran while one was open for 13% of the time, Pallas kernels for 0%

commit v1 on v0

--- a/solution.py
+++ b/solution.py
@@ -118,7 +118,12 @@
     outgoing = jnp.dot(by_token, normed, preferred_element_type=jnp.float32).astype(jnp.bfloat16)
     outgoing = outgoing.reshape(expert_count, slot_limit, D)
     arrived = lax.all_to_all(outgoing, "sp", split_axis=0, concat_axis=0, tiled=True)
-    gathered = lax.all_gather(arrived, "tp", axis=0, tiled=True)
+    ring = [arrived]
+    for hop in range(3):
+        ring.append(lax.ppermute(ring[-1], "tp", [(dev, (dev + 1) % 4) for dev in range(4)]))
+    gathered = jnp.roll(
+        jnp.concatenate(ring[::-1], axis=0), (lax.axis_index("tp") + 1) * ring[0].shape[0], axis=0
+    )
     expert_rows = gathered.reshape(-1, D)
     gate_value = jnp.dot(expert_rows, w_gate[0], preferred_element_type=jnp.float32)
     up_value = jnp.dot(expert_rows, w_up[0], preferred_element_type=jnp.float32)

time: 233 us -> 244 us (1.047)
  local copies, waits for them, and re-layouts: 18.3 us -> 27.3 us
  waiting for transfers between devices: 85.5 us -> 89.1 us
  matrix products: 34.5 us -> 31.8 us
    ppermute x0 -> x3, waiting for transfers between devices: none -> 26.2 us  [local(): lax.ppermute(ring[-1], 'tp', [(dev, (dev + 1) % 4) for dev in range(4)])]
    all_gather x1 -> x0, waiting for transfers between devices: 20.8 us -> none  [local(): gathered = lax.all_gather(arrived, 'tp', axis=0, tiled=True)]
    unnamed x18 -> x33, local copies, waits for them, and re-layouts: 1.14 us -> 9.82 us
    dot_general x1, matrix products: 4.45 us -> 1.81 us  [local(): jnp.dot(expert_rows, w_gate[0], preferred_element_type=jnp.float32)]
  transfers between devices with their start and end apart: 13 -> 15, of which waited for: 4 -> 6; matrix products, arithmetic and copies ran while one was open for 13% -> 13% of each run, Pallas kernels for 0% -> 0%
where the time goes in v1:
time: 244 us; the launch traced here: 242 us
  waiting for transfers between devices  89.1 us (37%)
  matrix products  31.8 us (13%)
  other arithmetic  31.5 us (13%)
  starting transfers between devices  30.1 us (12%)
  local copies, waits for them, and re-layouts  27.3 us (11%)
  blocking collectives  18.7 us (8%)
  between operations  13.6 us (6%)
    reduce_scatter x1, waiting for transfers between devices, local(): lax.psum_scatter(partial_out.reshape(tp_count, sp_count * slot_limit, D)....  29.5 us
    ppermute x3, waiting for transfers between devices, local(): lax.ppermute(ring[-1], 'tp', [(dev, (dev + 1) % 4) for dev in range(4)])  26.2 us
    ppermute x9, starting transfers between devices, passed_along(): lax.ppermute(value, axis, [(source, source + steps) for source in range(i...  25.2 us
    another operation x4, other arithmetic, attend_terms(): lax.cumsum(keep, axis=3, reverse=True) - keep + carried[:, :, :, None]  21.2 us
    reduce_scatter x1, waiting for transfers between devices, local(): lax.psum_scatter(jnp.dot(mixed, w_out, preferred_element_type=jnp.float32...  19 us
    all_to_all x1, blocking collectives, local(): lax.all_to_all(outgoing, 'sp', split_axis=0, concat_axis=0, tiled=True)  18.7 us
    all_to_all x1, waiting for transfers between devices, local(): lax.all_to_all(expert_result, 'sp', split_axis=0, concat_axis=0, tiled=True)  14.3 us
    dot_general x4, matrix products, attend_terms(): jnp.einsum('qgrd,sgd->grqs', query_grid, key_block.reshape(key_count, kv_...  10.4 us
  transfers between devices with their start and end apart: 15, of which 6 were waited for; matrix products, arithmetic and copies ran while one was open for 13% of the time, Pallas kernels for 0%

profile of v1, /device:TPU:0, one launch (start us, length us, event | category | flops | bytes accessed | tf_op | source)
XLA Modules:
  0.0 242.2 jit_solution(18398306935887122782)
XLA Ops:
  7.5 1.3 fusion.58
  8.8 1.5 reshape.106
  10.2 1.6 copy.62
  11.8 1.5 reshape.108
  13.3 1.6 copy.63
  15.9 1.3 add.170
  17.9 2.4 %fusion.56 = (f32[2,2,128]{2,1,0:T(2,128)}, f32[2,2,128,128]{2,3,1,0:T(8,128)S(1)}, f32[2,2,128,128]{2,3,1,0:T(8,128)}) fusion(pred[128,128]{0,1:T(8,128)(4,1)S(1)} %fusion.50, f32[2,2]{1,0:T(2,128)} %add.170, bf16[128,2,2,128]{0,3,2,1:T(8,128)(2,1)S(1)} %bitcast.80, bf16[128,2,128,1]{2,1,0,3:T(2,128)(2,1)} %bitcast.83), kind=kOutput, calls=%fused_computation.83 | convolution fusion | flops 17497600 | bytes 739344 | tf_op jit(solution)/shard_map/qgrd,sgd->grqs/dot_general | solution.py:23
  20.3 5.1 %reduce_window_sum.31 = f32[2,2,128,128]{2,3,1,0:T(8,128)} reduce-window(f32[2,2,128,128]{2,3,1,0:T(8,128)S(1)} %get-tuple-element.229, f32[]{:T(128)} %constant.78.clone.1), window={size=1x1x1x128 pad=0_0x0_0x0_0x0_127}, to_apply=%region_0.1 | reduce-window | flops 8323072 | bytes 524292 | tf_op jit(solution)/shard_map/attend_terms/reduce_window_sum | solution.py:33
  25.5 2.3 convolution_bitcast_fusion.1
  27.7 69.8 %while.21 = (s32[]{:T(128)}, f32[128,2,2,128]{3,0,2,1:T(8,128)}, f32[2,2,128]{2,1,0:T(2,128)}, bf16[128,256]{0,1:T(8,128)(2,1)}, bf16[128,256]{0,1:T(8,128)(2,1)...) while((s32[]{:T(128)}, f32[128,2,2,128]{3,0,2,1:T(8,128)}, ...), condition=%wide.region_5.6_spmd, body=%wide.region_2.5_spmd.sunk | while | flops 44105732 | bytes 3207487 | solution.py:87
  27.7 4.9 %collective-permute-start.1 = (bf16[128,1]{0,1:T(2,128)(2,1)}, bf16[128,1]{0,1:T(2,128)(2,1)S(1)}, u32[]{:S(2)}, u32[]{:S(2)}) collective-permute-start(bf16[128,1]{0,1:T(2,128)(2,1)} %get-tuple-element.318), channel_id=1, source_target_pairs={{0,4},{4,8},{8,12},{1,5},{5,9},{9,13},{2,6},{6,10},{10,14},{3,7},{... | collective-permute-start | bytes 776 | tf_op jit(solution)/shard_map/while/body/eval_jaxpr/ppermute | solution.py:16
  32.7 3.5 %collective-permute-start.2 = (bf16[128,256]{0,1:T(8,128)(2,1)}, bf16[128,256]{0,1:T(8,128)(2,1)S(1)}, u32[]{:S(2)}, u32[]{:S(2)}) collective-permute-start(bf16[128,256]{0,1:T(8,128)(2,1)} %get-tuple-element.316), channel_id=1, source_target_pairs={{0,4},{4,8},{8,12},{1,5},{5,9},{9,13},{2,6},{6,10},{10,14},{3,7},{... | collective-permute-start | bytes 196616 | tf_op jit(solution)/shard_map/while/body/eval_jaxpr/ppermute | solution.py:16
  36.2 3.5 %collective-permute-start = (bf16[128,256]{0,1:T(8,128)(2,1)}, bf16[128,256]{0,1:T(8,128)(2,1)S(1)}, u32[]{:S(2)}, u32[]{:S(2)}) collective-permute-start(bf16[128,256]{0,1:T(8,128)(2,1)} %get-tuple-element.317), channel_id=1, source_target_pairs={{0,4},{4,8},{8,12},{1,5},{5,9},{9,13},{2,6},{6,10},{10,14},{3,7},{... | collective-permute-start | bytes 196616 | tf_op jit(solution)/shard_map/while/body/eval_jaxpr/ppermute | solution.py:16
  41.7 2.6 %fusion.80 = (f32[2,2,128]{2,1,0:T(2,128)}, f32[2,2,128,128]{2,3,1,0:T(8,128)}, f32[2,2,128,128]{2,3,1,0:T(8,128)}) fusion(pred[128,128]{0,1:T(8,128)(4,1)S(1)} %compare_and_fusion.2, f32[2,2]{1,0:T(2,128)S(1)} %add.268, bf16[128,2,128,1]{0,2,3,1:T(8,128)(2,1)S(1)} %bitcast.76, bf16[128,2,2,128]{3,0,2,1:T(8,128)(2,1)} %get-tuple-element.334), kind=kOutput, calls=%fused_computation.19.clone.1 | convolution fusion | flops 17497600 | bytes 739344 | tf_op jit(solution)/shard_map/while/body/eval_jaxpr/qgrd,sgd->grqs/dot_general | solution.py:23
  44.3 5.4 %reduce_window_sum.34 = f32[2,2,128,128]{2,3,1,0:T(8,128)S(1)} reduce-window(f32[2,2,128,128]{2,3,1,0:T(8,128)} %get-tuple-element.297, f32[]{:T(128)} %constant.78.clone.1..sunk), window={size=1x1x1x128 pad=0_0x0_0x0_0x0_127}, to_apply=%region_3.3 | reduce-window | flops 8323072 | bytes 524292 | tf_op jit(solution)/shard_map/while/body/eval_jaxpr/reduce_window_sum | solution.py:33
  49.7 2.3 fusion.81
  52.0 1.3 add.269
  54.5 1.9 collective-permute-start.1
  56.4 2.6 %collective-permute-start.2 = (bf16[128,256]{0,1:T(8,128)(2,1)}, bf16[128,256]{0,1:T(8,128)(2,1)S(1)}, u32[]{:S(2)}, u32[]{:S(2)}) collective-permute-start(bf16[128,256]{0,1:T(8,128)(2,1)} %get-tuple-element.316), channel_id=1, source_target_pairs={{0,4},{4,8},{8,12},{1,5},{5,9},{9,13},{2,6},{6,10},{10,14},{3,7},{... | collective-permute-start | bytes 196616 | tf_op jit(solution)/shard_map/while/body/eval_jaxpr/ppermute | solution.py:16
  59.1 1.9 collective-permute-start
  63.0 2.6 %fusion.80 = (f32[2,2,128]{2,1,0:T(2,128)}, f32[2,2,128,128]{2,3,1,0:T(8,128)}, f32[2,2,128,128]{2,3,1,0:T(8,128)}) fusion(pred[128,128]{0,1:T(8,128)(4,1)S(1)} %compare_and_fusion.2, f32[2,2]{1,0:T(2,128)S(1)} %add.268, bf16[128,2,128,1]{0,2,3,1:T(8,128)(2,1)S(1)} %bitcast.76, bf16[128,2,2,128]{3,0,2,1:T(8,128)(2,1)} %get-tuple-element.334), kind=kOutput, calls=%fused_computation.19.clone.1 | convolution fusion | flops 17497600 | bytes 739344 | tf_op jit(solution)/shard_map/while/body/eval_jaxpr/qgrd,sgd->grqs/dot_general | solution.py:23
  65.6 5.4 %reduce_window_sum.34 = f32[2,2,128,128]{2,3,1,0:T(8,128)S(1)} reduce-window(f32[2,2,128,128]{2,3,1,0:T(8,128)} %get-tuple-element.297, f32[]{:T(128)} %constant.78.clone.1..sunk), window={size=1x1x1x128 pad=0_0x0_0x0_0x0_127}, to_apply=%region_3.3 | reduce-window | flops 8323072 | bytes 524292 | tf_op jit(solution)/shard_map/while/body/eval_jaxpr/reduce_window_sum | solution.py:33
  71.0 2.3 fusion.81
  73.3 1.3 add.269
  75.8 2.6 %collective-permute-start.1 = (bf16[128,1]{0,1:T(2,128)(2,1)}, bf16[128,1]{0,1:T(2,128)(2,1)S(1)}, u32[]{:S(2)}, u32[]{:S(2)}) collective-permute-start(bf16[128,1]{0,1:T(2,128)(2,1)} %get-tuple-element.318), channel_id=1, source_target_pairs={{0,4},{4,8},{8,12},{1,5},{5,9},{9,13},{2,6},{6,10},{10,14},{3,7},{... | collective-permute-start | bytes 776 | tf_op jit(solution)/shard_map/while/body/eval_jaxpr/ppermute | solution.py:16
  78.5 2.2 collective-permute-start.2
  80.7 2.0 collective-permute-start
  84.7 2.6 %fusion.80 = (f32[2,2,128]{2,1,0:T(2,128)}, f32[2,2,128,128]{2,3,1,0:T(8,128)}, f32[2,2,128,128]{2,3,1,0:T(8,128)}) fusion(pred[128,128]{0,1:T(8,128)(4,1)S(1)} %compare_and_fusion.2, f32[2,2]{1,0:T(2,128)S(1)} %add.268, bf16[128,2,128,1]{0,2,3,1:T(8,128)(2,1)S(1)} %bitcast.76, bf16[128,2,2,128]{3,0,2,1:T(8,128)(2,1)} %get-tuple-element.334), kind=kOutput, calls=%fused_computation.19.clone.1 | convolution fusion | flops 17497600 | bytes 739344 | tf_op jit(solution)/shard_map/while/body/eval_jaxpr/qgrd,sgd->grqs/dot_general | solution.py:23
  87.4 5.4 %reduce_window_sum.34 = f32[2,2,128,128]{2,3,1,0:T(8,128)S(1)} reduce-window(f32[2,2,128,128]{2,3,1,0:T(8,128)} %get-tuple-element.297, f32[]{:T(128)} %constant.78.clone.1..sunk), window={size=1x1x1x128 pad=0_0x0_0x0_0x0_127}, to_apply=%region_3.3 | reduce-window | flops 8323072 | bytes 524292 | tf_op jit(solution)/shard_map/while/body/eval_jaxpr/reduce_window_sum | solution.py:33
  92.7 2.3 fusion.81
  95.0 1.3 add.269
  97.5 1.1 copy.65
  98.7 2.9 %convolution_convert_fusion.1 = bf16[128,2048]{1,0:T(8,128)(2,1)} fusion(bf16[128,512]{0,1:T(8,128)(2,1)S(1)} %bitcast.81, bf16[512,2048]{1,0:T(8,128)(2,1)} %param.20), kind=kOutput, calls=%fused_computation.28 | convolution fusion | flops 268697600 | bytes 2752512 | tf_op jit(solution)/shard_map/dot_general | solution.py:92
  102.6 19.0 %reduce-scatter.3.cloned.1.call-done = bf16[32,2048]{1,0:T(8,128)(2,1)} async-done(((bf16[128,2048]{1,0:T(8,128)(2,1)}), bf16[32,2048]{1,0:T(8,128)(2,1)}) %reduce-scatter.3.cloned.1.call-update) | async-done | bytes 131088 | tf_op jit(solution)/shard_map/reduce_scatter | solution.py:91
  122.7 1.2 convolution_convert_fusion
  123.9 18.7 %all_to_all.10 = bf16[4,32,2048]{2,1,0:T(8,128)(2,1)S(1)} all-to-all(bf16[4,32,2048]{2,1,0:T(8,128)(2,1)S(1)} %bitcast.75), channel_id=1, replica_groups=mesh['grp'=2,'sp'=4,'tp'=4] {'sp'}, dimensions={0} | all-to-all | bytes 1048576 | tf_op jit(solution)/shard_map/all_to_all | solution.py:120
  143.5 8.6 %collective-permute-done.3 = bf16[4,32,2048]{2,1,0:T(8,128)(2,1)S(1)} collective-permute-done((bf16[4,32,2048]{2,1,0:T(8,128)(2,1)S(1)}, bf16[4,32,2048]{2,1,0:T(8,128)(2,1)S(1)}, u32[]{:S(2)}, u32[]{:S(2)}) %collective-permute-start.3) | collective-permute-done | bytes 524320 | tf_op jit(solution)/shard_map/ppermute | solution.py:123
  152.9 8.7 %collective-permute-done.4 = bf16[4,32,2048]{2,1,0:T(8,128)(2,1)} collective-permute-done((bf16[4,32,2048]{2,1,0:T(8,128)(2,1)S(1)}, bf16[4,32,2048]{2,1,0:T(8,128)(2,1)}, u32[]{:S(2)}, u32[]{:S(2)}) %collective-permute-start.4) | collective-permute-done | bytes 524320 | tf_op jit(solution)/shard_map/ppermute | solution.py:123
  161.6 8.9 %collective-permute-done.5 = bf16[4,32,2048]{2,1,0:T(8,128)(2,1)} collective-permute-done((bf16[4,32,2048]{2,1,0:T(8,128)(2,1)}, bf16[4,32,2048]{2,1,0:T(8,128)(2,1)}, u32[]{:S(2)}, u32[]{:S(2)}) %collective-permute-start.5) | collective-permute-done | bytes 524320 | tf_op jit(solution)/shard_map/ppermute | solution.py:123
  171.6 1.1 constant_dynamic-update-slice_fusion.6
  176.3 1.5 copy-done.10
  177.9 1.8 fusion.21
  179.7 1.9 multiply_convert_fusion
  181.7 3.2 %fusion.23 = bf16[4,128,2048]{2,1,0:T(8,128)(2,1)} fusion(bf16[4,128,768]{2,1,0:T(8,128)(2,1)S(1)} %bitcast.85, bf16[1,768,2048]{2,1,0:T(8,128)(2,1)S(1)} %copy-done), kind=kOutput, calls=%fused_computation.26 | convolution fusion | flops 1611661312 | bytes 6029312 | tf_op jit(solution)/shard_map/dot_general | solution.py:131
  184.9 29.5 %reduce-scatter.5.cloned.1.call-done = bf16[1,128,2048]{2,1,0:T(8,128)(2,1)} async-done(((bf16[4,128,2048]{2,1,0:T(8,128)(2,1)}), bf16[1,128,2048]{2,1,0:T(8,128)(2,1)}) %reduce-scatter.5.cloned.1.call-update) | async-done | bytes 524304 | tf_op jit(solution)/shard_map/reduce_scatter | solution.py:132
  214.4 4.6 %all-to-all-start.1 = ((bf16[4,32,2048]{2,1,0:T(8,128)(2,1)}), bf16[4,32,2048]{2,1,0:T(8,128)(2,1)}, u32[]{:S(2)}, u32[]{:S(2)}) async-start(bf16[4,32,2048]{2,1,0:T(8,128)(2,1)} %bitcast.78), calls=%async_computation.3 | async-start | bytes 1048576 | tf_op jit(solution)/shard_map/all_to_all | solution.py:139
  219.1 14.3 %all-to-all-done.1 = bf16[4,32,2048]{2,1,0:T(8,128)(2,1)} async-done(((bf16[4,32,2048]{2,1,0:T(8,128)(2,1)}), bf16[4,32,2048]{2,1,0:T(8,128)(2,1)}, u32[]{:S(2)}, u32[]{:S(2)}) %all-to-all-start.1) | async-done | bytes 524320 | tf_op jit(solution)/shard_map/all_to_all | solution.py:139
  233.4 1.3 fusion.28
  (80 shorter events, 21.7 us)
Async XLA Ops:
  6.5 175.1 %copy-start = (bf16[1,768,2048]{2,1,0:T(8,128)(2,1)S(1)}, bf16[1,768,2048]{2,1,0:T(8,128)(2,1)}, u32[]{:S(2)}) copy-start(bf16[1,768,2048]{2,1,0:T(8,128)(2,1)} %param.27) | copy-start | bytes 9437188
  6.5 115.0 %reduce-scatter.3.cloned.1.call-start = ((), (), s32[]{:S(2)}) async-start(), calls=%async_computation.4 | async-start | bytes 655360 | tf_op jit(solution)/shard_map/reduce_scatter | solution.py:91
  27.7 12.7 %collective-permute-start.1 = (bf16[128,1]{0,1:T(2,128)(2,1)}, bf16[128,1]{0,1:T(2,128)(2,1)S(1)}, u32[]{:S(2)}, u32[]{:S(2)}) collective-permute-start(bf16[128,1]{0,1:T(2,128)(2,1)} %get-tuple-element.318), channel_id=1, source_target_pairs={{0,4},{4,8},{8,12},{1,5},{5,9},{9,13},{2,6},{6,10},{10,14},{3,7},{... | collective-permute-start | bytes 776 | tf_op jit(solution)/shard_map/while/body/eval_jaxpr/ppermute | solution.py:16
  32.7 9.0 %collective-permute-start.2 = (bf16[128,256]{0,1:T(8,128)(2,1)}, bf16[128,256]{0,1:T(8,128)(2,1)S(1)}, u32[]{:S(2)}, u32[]{:S(2)}) collective-permute-start(bf16[128,256]{0,1:T(8,128)(2,1)} %get-tuple-element.316), channel_id=1, source_target_pairs={{0,4},{4,8},{8,12},{1,5},{5,9},{9,13},{2,6},{6,10},{10,14},{3,7},{... | collective-permute-start | bytes 196616 | tf_op jit(solution)/shard_map/while/body/eval_jaxpr/ppermute | solution.py:16
  36.2 13.5 %collective-permute-start = (bf16[128,256]{0,1:T(8,128)(2,1)}, bf16[128,256]{0,1:T(8,128)(2,1)S(1)}, u32[]{:S(2)}, u32[]{:S(2)}) collective-permute-start(bf16[128,256]{0,1:T(8,128)(2,1)} %get-tuple-element.317), channel_id=1, source_target_pairs={{0,4},{4,8},{8,12},{1,5},{5,9},{9,13},{2,6},{6,10},{10,14},{3,7},{... | collective-permute-start | bytes 196616 | tf_op jit(solution)/shard_map/while/body/eval_jaxpr/ppermute | solution.py:16
  54.5 7.2 %collective-permute-start.1 = (bf16[128,1]{0,1:T(2,128)(2,1)}, bf16[128,1]{0,1:T(2,128)(2,1)S(1)}, u32[]{:S(2)}, u32[]{:S(2)}) collective-permute-start(bf16[128,1]{0,1:T(2,128)(2,1)} %get-tuple-element.318), channel_id=1, source_target_pairs={{0,4},{4,8},{8,12},{1,5},{5,9},{9,13},{2,6},{6,10},{10,14},{3,7},{... | collective-permute-start | bytes 776 | tf_op jit(solution)/shard_map/while/body/eval_jaxpr/ppermute | solution.py:16
  56.4 6.6 %collective-permute-start.2 = (bf16[128,256]{0,1:T(8,128)(2,1)}, bf16[128,256]{0,1:T(8,128)(2,1)S(1)}, u32[]{:S(2)}, u32[]{:S(2)}) collective-permute-start(bf16[128,256]{0,1:T(8,128)(2,1)} %get-tuple-element.316), channel_id=1, source_target_pairs={{0,4},{4,8},{8,12},{1,5},{5,9},{9,13},{2,6},{6,10},{10,14},{3,7},{... | collective-permute-start | bytes 196616 | tf_op jit(solution)/shard_map/while/body/eval_jaxpr/ppermute | solution.py:16
  59.1 12.0 %collective-permute-start = (bf16[128,256]{0,1:T(8,128)(2,1)}, bf16[128,256]{0,1:T(8,128)(2,1)S(1)}, u32[]{:S(2)}, u32[]{:S(2)}) collective-permute-start(bf16[128,256]{0,1:T(8,128)(2,1)} %get-tuple-element.317), channel_id=1, source_target_pairs={{0,4},{4,8},{8,12},{1,5},{5,9},{9,13},{2,6},{6,10},{10,14},{3,7},{... | collective-permute-start | bytes 196616 | tf_op jit(solution)/shard_map/while/body/eval_jaxpr/ppermute | solution.py:16
  75.8 7.6 %collective-permute-start.1 = (bf16[128,1]{0,1:T(2,128)(2,1)}, bf16[128,1]{0,1:T(2,128)(2,1)S(1)}, u32[]{:S(2)}, u32[]{:S(2)}) collective-permute-start(bf16[128,1]{0,1:T(2,128)(2,1)} %get-tuple-element.318), channel_id=1, source_target_pairs={{0,4},{4,8},{8,12},{1,5},{5,9},{9,13},{2,6},{6,10},{10,14},{3,7},{... | collective-permute-start | bytes 776 | tf_op jit(solution)/shard_map/while/body/eval_jaxpr/ppermute | solution.py:16
  78.5 6.2 %collective-permute-start.2 = (bf16[128,256]{0,1:T(8,128)(2,1)}, bf16[128,256]{0,1:T(8,128)(2,1)S(1)}, u32[]{:S(2)}, u32[]{:S(2)}) collective-permute-start(bf16[128,256]{0,1:T(8,128)(2,1)} %get-tuple-element.316), channel_id=1, source_target_pairs={{0,4},{4,8},{8,12},{1,5},{5,9},{9,13},{2,6},{6,10},{10,14},{3,7},{... | collective-permute-start | bytes 196616 | tf_op jit(solution)/shard_map/while/body/eval_jaxpr/ppermute | solution.py:16
  80.7 12.1 %collective-permute-start = (bf16[128,256]{0,1:T(8,128)(2,1)}, bf16[128,256]{0,1:T(8,128)(2,1)S(1)}, u32[]{:S(2)}, u32[]{:S(2)}) collective-permute-start(bf16[128,256]{0,1:T(8,128)(2,1)} %get-tuple-element.317), channel_id=1, source_target_pairs={{0,4},{4,8},{8,12},{1,5},{5,9},{9,13},{2,6},{6,10},{10,14},{3,7},{... | collective-permute-start | bytes 196616 | tf_op jit(solution)/shard_map/while/body/eval_jaxpr/ppermute | solution.py:16
  97.5 4.2 %copy-start.8 = (s32[32,2]{0,1:T(2,128)S(1)}, s32[32,2]{0,1:T(2,128)}, u32[]{:S(2)}) copy-start(s32[32,2]{0,1:T(2,128)} %param.23) | copy-start | bytes 772
  97.5 24.0 %copy-start.5 = (bf16[32,2048]{1,0:T(8,128)(2,1)S(1)}, bf16[32,2048]{1,0:T(8,128)(2,1)}, u32[]{:S(2)}) copy-start(bf16[32,2048]{1,0:T(8,128)(2,1)} %param.21) | copy-start | bytes 393220
  97.5 25.1 %copy-start.7 = (f32[2048]{0:T(1024)S(1)}, f32[2048]{0:T(1024)}, u32[]{:S(2)}) copy-start(f32[2048]{0:T(1024)} %param.22) | copy-start | bytes 24580
  101.5 112.8 %reduce-scatter.5.cloned.1.call-start = ((), (), s32[]{:S(2)}) async-start(), calls=%async_computation.5 | async-start | bytes 2621440 | tf_op jit(solution)/shard_map/reduce_scatter | solution.py:132
  142.6 0.8 copy-start.1
  143.5 8.6 %collective-permute-start.3 = (bf16[4,32,2048]{2,1,0:T(8,128)(2,1)S(1)}, bf16[4,32,2048]{2,1,0:T(8,128)(2,1)S(1)}, u32[]{:S(2)}, u32[]{:S(2)}) collective-permute-start(bf16[4,32,2048]{2,1,0:T(8,128)(2,1)S(1)} %all_to_all.10), channel_id=1, source_target_pairs={{0,1},{1,2},{2,3},{3,0},{4,5},{5,6},{6,7},{7,4},{8,9},{9,10},{10,1... | collective-permute-start | bytes 1572872 | tf_op jit(solution)/shard_map/ppermute | solution.py:123
  152.1 0.8 copy-start.3
  152.9 8.7 %collective-permute-start.4 = (bf16[4,32,2048]{2,1,0:T(8,128)(2,1)S(1)}, bf16[4,32,2048]{2,1,0:T(8,128)(2,1)}, u32[]{:S(2)}, u32[]{:S(2)}) collective-permute-start(bf16[4,32,2048]{2,1,0:T(8,128)(2,1)S(1)} %collective-permute-done.3), channel_id=1, source_target_pairs={{0,1},{1,2},{2,3},{3,0},{4,5},{5,6},{6,7},{7,4},{8,9},{9,10},{10,1... | collective-permute-start | bytes 1572872 | tf_op jit(solution)/shard_map/ppermute | solution.py:123
  161.6 8.9 %collective-permute-start.5 = (bf16[4,32,2048]{2,1,0:T(8,128)(2,1)}, bf16[4,32,2048]{2,1,0:T(8,128)(2,1)}, u32[]{:S(2)}, u32[]{:S(2)}) collective-permute-start(bf16[4,32,2048]{2,1,0:T(8,128)(2,1)} %collective-permute-done.4), channel_id=1, source_target_pairs={{0,1},{1,2},{2,3},{3,0},{4,5},{5,6},{6,7},{7,4},{8,9},{9,10},{10,1... | collective-permute-start | bytes 1572872 | tf_op jit(solution)/shard_map/ppermute | solution.py:123
  161.6 12.2 %copy-start.2 = (bf16[4,32,2048]{2,1,0:T(8,128)(2,1)S(1)}, bf16[4,32,2048]{2,1,0:T(8,128)(2,1)}, u32[]{:S(2)}) copy-start(bf16[4,32,2048]{2,1,0:T(8,128)(2,1)} %copy-done.1) | copy-start | bytes 1572868
  161.6 14.4 %copy-start.4 = (bf16[4,32,2048]{2,1,0:T(8,128)(2,1)S(1)}, bf16[4,32,2048]{2,1,0:T(8,128)(2,1)}, u32[]{:S(2)}) copy-start(bf16[4,32,2048]{2,1,0:T(8,128)(2,1)} %copy-done.3) | copy-start | bytes 1572868
  176.0 1.9 copy-start.10
  177.9 1.9 copy-start.11
  184.9 48.5 %copy-start.9 = (f32[32,2]{0,1:T(2,128)S(1)}, f32[32,2]{0,1:T(2,128)}, u32[]{:S(2)}) copy-start(f32[32,2]{0,1:T(2,128)} %param.24) | copy-start | bytes 772
  184.9 49.8 %copy-start.6 = (bf16[32,2048]{1,0:T(8,128)(2,1)S(1)}, bf16[32,2048]{1,0:T(8,128)(2,1)}, u32[]{:S(2)}) copy-start(bf16[32,2048]{1,0:T(8,128)(2,1)} %reduce-scatter.3.cloned.1.call-done) | copy-start | bytes 393220
  214.4 19.0 %all-to-all-start.1 = ((bf16[4,32,2048]{2,1,0:T(8,128)(2,1)}), bf16[4,32,2048]{2,1,0:T(8,128)(2,1)}, u32[]{:S(2)}, u32[]{:S(2)}) async-start(bf16[4,32,2048]{2,1,0:T(8,128)(2,1)} %bitcast.78), calls=%async_computation.3 | async-start | bytes 1048576 | tf_op jit(solution)/shard_map/all_to_all | solution.py:139
Sparse Core Ops, SparseCore 0:
  101.7 19.8 reduce-scatter.2
  185.0 29.3 reduce-scatter.4
